TPU v7x, 32 devices: a whole 2x2x4 slice. The times are simulated.
32 devices in a mesh: ep: 4 (over y, x), tp: 8 (over z, core).
Axes of the slice: x: 2, y: 2, z: 4, core: 2. Of those that a mesh axis runs over, the one named last changes fastest.
Arguments:
- tokens: bfloat16 [64, 2048], P('ep'), may hold values from -6 to 6
- routes: int32 [64, 4], P('ep'), may hold values from 0 to 7, all different within a row; in each aligned block of 16 rows (0 to 15, 16 to 31, ...) at most 16 rows name the same one
- route_weight: float32 [64, 4], P('ep'), may hold values from 0.2 to 1
- mixer_gain: float32 [2048], replicated, may hold values from 0.1 to 1.9
- gate_weight: bfloat16 [2048, 4096], P(None, 'tp'), may hold values from -0.125 to 0.125
- input_weight: bfloat16 [2048, 4096], P(None, 'tp'), may hold values from -0.125 to 0.125
- step_weight: bfloat16 [2048, 64], P(None, 'tp'), may hold values from -0.125 to 0.125
- write_weight: bfloat16 [2048, 512], P('tp'), may hold values from -0.125 to 0.125
- read_weight: bfloat16 [2048, 512], P('tp'), may hold values from -0.125 to 0.125
- step_bias: float32 [64], P('tp'), may hold values from -3 to 0.5
- decay_log: float32 [64], P('tp'), may hold values from -2 to 0.5
- decay_jolt: float32 [64, 64], P('ep', 'tp'), may hold values from -1 to 0
- filter_taps: bfloat16 [4, 4096], P(None, 'tp'), may hold values from -3 to 3
- filter_state: bfloat16 [64, 3, 4096], P('ep', None, 'tp'), may hold values from -6 to 6
- scan_state: float32 [64, 64, 64, 128], P('ep', 'tp'), may hold values from -2 to 2
- skip_gain: float32 [64], P('tp'), may hold values from 0.5 to 2
- head_gain: float32 [4096], P('tp'), may hold values from 0.1 to 1.9
- output_weight: bfloat16 [4096, 2048], P('tp'), may hold values from -0.09375 to 0.09375
- channel_gain: float32 [2048], replicated, may hold values from 0.1 to 1.9
- expert_gate: bfloat16 [8, 2048, 2048], P('ep', None, 'tp'), may hold values from -0.125 to 0.125
- expert_up: bfloat16 [8, 2048, 2048], P('ep', None, 'tp'), may hold values from -0.125 to 0.125
- expert_down: bfloat16 [8, 2048, 2048], P('ep', 'tp'), may hold values from -0.125 to 0.125
- shared_gate: bfloat16 [2048, 2048], P(None, 'tp'), may hold values from -0.125 to 0.125
- shared_up: bfloat16 [2048, 2048], P(None, 'tp'), may hold values from -0.125 to 0.125
- shared_down: bfloat16 [2048, 2048], P('tp'), may hold values from -0.125 to 0.125
Outputs:
- layer_out: bfloat16 [64, 2048], P('ep', 'tp')
- new_state: float32 [64, 64, 64, 128], P('ep', 'tp')
- new_filter: bfloat16 [64, 3, 4096], P('ep', None, 'tp')
Inputs may be any that keep to these rules, and one draw needn't show every extreme that they name: `routes`: each row names 4 different experts. In each aligned block of 16 rows (the rows of one index of ep) no expert is named by more than 16 rows, a bound that some block reaches.
All inputs are finite; a program needn't handle non-finite values.
Results may differ from a plain program's by a relative error of at most 0.025.
Values may be sent and summed in bfloat16 or wider, within the bound.
A program may use at most 64 MiB of HBM per device.

v0:
```python
import jax
import jax.numpy as jnp
from jax import lax
from jax.sharding import PartitionSpec as P

HEADS = 64
HEAD_DIM = 64
GROUPS = 4
STATE = 128
EPS = 1e-06


def rms_normed(values, scaling):
    mean_square = jnp.mean(values * values, axis=-1, keepdims=True)
    return values * lax.rsqrt(mean_square + EPS) * scaling


def route_targets(route_ids, experts, capacity):
    count_rows, top_picks = route_ids.shape
    flattened = route_ids.reshape(count_rows * top_picks)
    onehot = (flattened[:, None] == jnp.arange(experts, dtype=jnp.int32)[None, :]).astype(jnp.int32)
    before = jnp.cumsum(onehot, axis=0) - onehot
    slot_index = jnp.sum(before * onehot, axis=1)
    return (flattened * capacity + slot_index).reshape(count_rows, top_picks)


def expert_terms(token_rows, expert_gate, expert_up, expert_down):
    gate_part = jnp.einsum(
        "ajcd,jdf->ajcf", token_rows, expert_gate, preferred_element_type=jnp.float32
    )
    up_part = jnp.einsum(
        "ajcd,jdf->ajcf", token_rows, expert_up, preferred_element_type=jnp.float32
    )
    hidden = (jax.nn.silu(gate_part) * up_part).astype(jnp.bfloat16)
    return jnp.einsum("ajcf,jfd->ajcd", hidden, expert_down, preferred_element_type=jnp.float32)


def on_device(
    tokens,
    routes,
    route_weight,
    mixer_gain,
    gate_weight,
    input_weight,
    step_weight,
    write_weight,
    read_weight,
    step_bias,
    decay_log,
    decay_jolt,
    filter_taps,
    filter_state,
    scan_state,
    skip_gain,
    head_gain,
    output_weight,
    channel_gain,
    expert_gate,
    expert_up,
    expert_down,
    shared_gate,
    shared_up,
    shared_down,
):
    seq_rows, model_width = tokens.shape
    tp_count = lax.axis_size("tp")
    tp_index = lax.axis_index("tp")
    ep_count = lax.axis_size("ep")
    col_count = model_width // tp_count
    col_start = tp_index * col_count
    tokens_f = tokens.astype(jnp.float32)
    normed = rms_normed(tokens_f, mixer_gain).astype(jnp.bfloat16)
    feature_rows = write_weight.shape[0]
    own_features = lax.dynamic_slice_in_dim(normed, tp_index * feature_rows, feature_rows, 1)
    write_part = jnp.dot(own_features, write_weight, preferred_element_type=jnp.float32)
    read_part = jnp.dot(own_features, read_weight, preferred_element_type=jnp.float32)
    write_in, read_in = (
        lax.psum(write_part.astype(jnp.bfloat16), "tp").astype(jnp.float32),
        lax.psum(read_part.astype(jnp.bfloat16), "tp").astype(jnp.float32),
    )
    gate_rows = jnp.dot(normed, gate_weight, preferred_element_type=jnp.float32).astype(
        jnp.bfloat16
    )
    input_rows = jnp.dot(normed, input_weight, preferred_element_type=jnp.float32).astype(
        jnp.bfloat16
    )
    step_raw = jnp.dot(normed, step_weight, preferred_element_type=jnp.float32)
    window = jnp.concatenate([filter_state, input_rows[:, None, :]], axis=1)
    filtered = jax.nn.silu(
        jnp.sum(window.astype(jnp.float32) * filter_taps.astype(jnp.float32)[None], axis=1)
    )
    step_size = jax.nn.softplus(step_raw + step_bias)
    log_decay = decay_jolt - jnp.exp(decay_log) * step_size
    heads_here = step_bias.shape[0]
    head_input = filtered.reshape(seq_rows, heads_here, HEAD_DIM)
    group_index = tp_index * heads_here // (HEADS // GROUPS)
    write_vec = jax.nn.silu(lax.dynamic_slice_in_dim(write_in, group_index * STATE, STATE, 1))
    read_vec = jax.nn.silu(lax.dynamic_slice_in_dim(read_in, group_index * STATE, STATE, 1))
    new_state = (
        jnp.exp(log_decay)[:, :, None, None] * scan_state
        + (step_size[:, :, None] * head_input)[:, :, :, None] * write_vec[:, None, None, :]
    )
    readout = jnp.einsum("shpn,sn->shp", new_state, read_vec, precision=lax.Precision.HIGHEST)
    readout = readout + skip_gain[None, :, None] * head_input
    gate_heads = gate_rows.astype(jnp.float32).reshape(seq_rows, heads_here, HEAD_DIM)
    gated = rms_normed(readout * jax.nn.silu(gate_heads), head_gain.reshape(heads_here, HEAD_DIM))
    gated = gated.astype(jnp.bfloat16).reshape(seq_rows, heads_here * HEAD_DIM)
    mixer_part = jnp.dot(gated, output_weight, preferred_element_type=jnp.float32)
    mixed = lax.psum(mixer_part.astype(jnp.bfloat16), "tp")
    resid = (tokens_f + mixed.astype(jnp.float32)).astype(jnp.bfloat16)
    normed_ffn = rms_normed(resid.astype(jnp.float32), channel_gain).astype(jnp.bfloat16)
    resid_own = lax.dynamic_slice_in_dim(resid, col_start, col_count, 1)
    shared_hidden = (
        jax.nn.silu(jnp.dot(normed_ffn, shared_gate, preferred_element_type=jnp.float32))
        * jnp.dot(normed_ffn, shared_up, preferred_element_type=jnp.float32)
    ).astype(jnp.bfloat16)
    shared_part = jnp.dot(shared_hidden, shared_down, preferred_element_type=jnp.float32)
    local_experts = expert_gate.shape[0]
    experts = local_experts * ep_count
    top_picks = routes.shape[1]
    capacity = 2 * seq_rows * top_picks // experts
    targets = route_targets(routes, experts, capacity)
    slot_ids = jnp.arange(experts * capacity, dtype=jnp.int32)
    dispatch = jnp.sum((targets[None, :, :] == slot_ids[:, None, None]).astype(jnp.float32), axis=2)
    send_rows = jnp.dot(
        dispatch.astype(jnp.bfloat16), normed_ffn, preferred_element_type=jnp.float32
    )
    send_rows = send_rows.astype(jnp.bfloat16).reshape(
        ep_count, local_experts, capacity, model_width
    )
    terms = expert_terms(
        lax.all_to_all(send_rows, "ep", split_axis=0, concat_axis=0, tiled=True),
        expert_gate,
        expert_up,
        expert_down,
    )
    routed_parts, shared_sum = (
        lax.psum_scatter(terms.astype(jnp.bfloat16), "tp", scatter_dimension=3, tiled=True).astype(
            jnp.float32
        ),
        lax.psum_scatter(
            shared_part.reshape(1, 1, seq_rows, model_width).astype(jnp.bfloat16),
            "tp",
            scatter_dimension=3,
            tiled=True,
        ).astype(jnp.float32),
    )
    expert_rows = routed_parts.astype(jnp.bfloat16)
    returned = lax.all_to_all(expert_rows, "ep", split_axis=0, concat_axis=0, tiled=True)
    returned = returned.reshape(experts * capacity, col_count).astype(jnp.float32)
    combine = jnp.sum(
        jnp.where(targets[:, :, None] == slot_ids[None, None, :], route_weight[:, :, None], 0.0),
        axis=1,
    )
    routed_sum = jnp.dot(combine, returned, precision=lax.Precision.HIGHEST)
    layer_out = (resid_own.astype(jnp.float32) + shared_sum[0, 0] + routed_sum).astype(jnp.bfloat16)
    return (layer_out, new_state, window[:, 1:, :])


def solution(mesh):
    in_specs = (
        P("ep", None),
        P("ep", None),
        P("ep", None),
        P(),
        P(None, "tp"),
        P(None, "tp"),
        P(None, "tp"),
        P("tp", None),
        P("tp", None),
        P("tp"),
        P("tp"),
        P("ep", "tp"),
        P(None, "tp"),
        P("ep", None, "tp"),
        P("ep", "tp", None, None),
        P("tp"),
        P("tp"),
        P("tp", None),
        P(),
        P("ep", None, "tp"),
        P("ep", None, "tp"),
        P("ep", "tp", None),
        P(None, "tp"),
        P(None, "tp"),
        P("tp", None),
    )
    out_specs = (P("ep", "tp"), P("ep", "tp", None, None), P("ep", None, "tp"))
    return jax.shard_map(
        on_device, mesh=mesh, in_specs=in_specs, out_specs=out_specs, check_vma=False
    )
```

profile of v0, /device:TPU:0, one launch (start us, length us, event | category | flops | bytes accessed | tf_op | source)
XLA Modules:
  0.0 199.6 jit_solution(1012858224445261043)
XLA Ops:
  7.2 0.0 all-reduce.3.cloned.1.call-start
  7.3 1.1 fusion.31
  8.4 0.9 fusion.33
  9.4 2.0 fusion.21
  11.4 0.1 reshape.93
  11.5 0.1 convolution_convert_fusion.6
  11.6 0.2 convolution_convert_fusion.5
  11.8 0.1 subtract_exponential_fusion
  11.9 0.1 copy.59
  12.0 2.0 fusion.22
  14.1 0.1 reduce_sum.69
  14.1 0.1 copy.58
  14.2 0.1 mul.206
  14.3 30.3 %all-reduce = (bf16[16,512]{1,0:T(8,128)(2,1)S(1)}, bf16[16,512]{1,0:T(8,128)(2,1)S(1)}) all-reduce(bf16[16,512]{1,0:T(8,128)(2,1)S(1)} %convolution_convert_fusion.6, bf16[16,512]{1,0:T(8,128)(2,1)S(1)} %convolution_convert_fusion.5), channel_id=1, replica_groups=mesh['ep'=4,'tp'=8] {'tp'}, use_global_device_ids=true, to_apply=%region_2.0 | all-reduce | flops 16384 | bytes 65536 | tf_op jit(solution)/shard_map/psum | solution.py:78
  44.6 0.1 broadcast_multiply_fusion
  44.7 3.1 %multiply_add_fusion = f32[16,8,64,128]{3,2,1,0:T(8,128)S(1)} fusion(f32[16,8,64,128]{3,2,1,0:T(8,128)} %param.39, f32[16,128]{1,0:T(8,128)S(1)} %get-tuple-element.12, f32[16,8,64]{2,1,0:T(8,128)S(1)} %broadcast_multiply_fusion, f32[16,8]{1,0:T(8,128)S(1)} %copy.58), kind=kLoop, calls=%fused_computation | loop fusion | flops 3145728 | bytes 8430080 | tf_op jit(solution)/shard_map/add | solution.py:100
  47.8 9.8 %fusion.68 = f32[16,1,8,64]{3,1,2,0:T(1,128)S(1)} fusion(f32[16,8,64,128]{3,2,1,0:T(8,128)S(1)} %multiply_add_fusion, f32[16,128,1,1]{1,2,3,0:T(1,128)S(1)} %bitcast.72), kind=kOutput, calls=%fused_computation.95 | convolution fusion | flops 12582912 | bytes 4235264 | tf_op jit(solution)/shard_map/shpn,sn->shp/dot_general | solution.py:103
  57.6 0.0 copy-start.2
  57.7 0.2 multiply_reduce_fusion.1
  57.9 0.1 multiply_convert_fusion
  58.0 0.1 reshape.89
  58.1 2.6 %convolution_convert_fusion.3 = bf16[16,2048]{1,0:T(8,128)(2,1)} fusion(bf16[16,512]{1,0:T(8,128)(2,1)S(1)} %reshape.89, bf16[512,2048]{1,0:T(8,128)(2,1)} %param.42), kind=kOutput, calls=%fused_computation.5 | convolution fusion | flops 33587200 | bytes 2179072 | tf_op jit(solution)/shard_map/dot_general | solution.py:108
  60.7 0.0 all-reduce.3.cloned.1.call-update
  60.7 0.0 reduce-scatter.5.cloned.1.call-start
  60.7 0.1 copy.60
  60.8 0.1 eq.20
  60.9 0.1 fusion.42
  61.0 0.1 reduce_window_sum.11
  61.1 0.2 select_reduce_fusion.1
  61.3 0.1 reduce_sum.73
  61.4 0.1 copy.61
  61.5 0.1 convert_reduce_fusion
  61.5 52.3 %all-reduce.3.cloned.1.call-done = bf16[16,2048]{1,0:T(8,128)(2,1)} async-done(((bf16[16,2048]{1,0:T(8,128)(2,1)}), bf16[16,2048]{1,0:T(8,128)(2,1)}) %all-reduce.3.cloned.1.call-update) | async-done | bytes 65552 | tf_op jit(solution)/shard_map/psum | solution.py:109
  113.9 1.0 fusion.28
  114.9 0.3 convolution_convert_fusion.1
  115.2 10.6 %all_to_all.10 = bf16[4,2,16,2048]{3,2,1,0:T(8,128)(2,1)S(1)} all-to-all(bf16[4,2,16,2048]{3,2,1,0:T(8,128)(2,1)S(1)} %bitcast.69), channel_id=1, replica_groups=mesh['ep'=4,'tp'=8] {'ep'}, dimensions={0} | all-to-all | bytes 1048576 | tf_op jit(solution)/shard_map/all_to_all | solution.py:132
  125.8 2.1 %fusion.7 = f32[4,2,16,256]{3,2,0,1:T(8,128)S(1)} fusion(bf16[2,2048,256]{2,1,0:T(8,128)(2,1)} %param.44, bf16[4,2,16,2048]{3,2,1,0:T(8,128)(2,1)S(1)} %all_to_all.10), kind=kOutput, calls=%fused_computation.12 | convolution fusion | flops 134217728 | bytes 2752512 | tf_op jit(solution)/shard_map/ajcd,jdf->ajcf/dot_general | solution.py:28
  127.8 3.3 %fusion = bf16[4,2,16,2048]{3,2,0,1:T(8,128)(2,1)} fusion(bf16[2,256,2048]{2,1,0:T(8,128)(2,1)S(1)} %copy-done, bf16[2,2048,256]{2,1,0:T(8,128)(2,1)} %param.45, bf16[4,2,16,2048]{3,2,1,0:T(8,128)(2,1)S(1)} %all_to_all.10, f32[4,2,16,256]{3,2,0,1:T(8,128)S(1)} %fusion.7), kind=kOutput, calls=%fused_computation.3 | convolution fusion | flops 268894208 | bytes 5373952 | tf_op jit(solution)/shard_map/ajcf,jfd->ajcd/dot_general | solution.py:35
  131.1 0.0 reduce-scatter.3.cloned.1.call-start
  131.2 1.5 fusion.65
  132.7 2.9 %fusion.1 = bf16[1,1,16,2048]{3,2,1,0:T(8,128)(2,1)} fusion(bf16[256,2048]{1,0:T(8,128)(2,1)} %param.49, bf16[2048,256]{1,0:T(8,128)(2,1)} %param.48, f32[16,256]{1,0:T(8,128)S(1)} %fusion.65, bf16[16,2048]{1,0:T(8,128)(2,1)S(1)} %get-tuple-element.6, f32[2048]{0:T(1024)S(1)} %copy-done.6, f32[16]{0:T(128)S(1)} %add_rsqrt_fusion.1), kind=kOutput, calls=%fused_computation.6 | convolution fusion | flops 33742848 | bytes 2252864 | tf_op jit(solution)/shard_map/dot_general | solution.py:117
  135.7 0.1 select_reduce_fusion
  135.8 25.0 %reduce-scatter.5.cloned.1.call-done = bf16[4,2,16,256]{3,2,0,1:T(8,128)(2,1)} async-done(((bf16[4,2,16,2048]{3,2,0,1:T(8,128)(2,1)}), bf16[4,2,16,256]{3,2,0,1:T(8,128)(2,1)}) %reduce-scatter.5.cloned.1.call-update) | async-done | bytes 65552 | tf_op jit(solution)/shard_map/reduce_scatter | solution.py:138
  160.8 1.5 copy.64
  162.2 3.6 %all-to-all-start.1 = ((bf16[4,2,16,256]{3,2,1,0:T(8,128)(2,1)}), bf16[4,2,16,256]{3,2,1,0:T(8,128)(2,1)S(1)}, u32[]{:S(2)}, u32[]{:S(2)}) async-start(bf16[4,2,16,256]{3,2,1,0:T(8,128)(2,1)} %copy.64), calls=%async_computation.3 | async-start | bytes 131072 | tf_op jit(solution)/shard_map/all_to_all | solution.py:149
  165.9 0.6 fusion.41
  166.5 25.2 %reduce-scatter.3.cloned.1.call-done = bf16[1,1,16,256]{3,2,1,0:T(8,128)(2,1)} async-done(((bf16[1,1,16,2048]{3,2,1,0:T(8,128)(2,1)}), bf16[1,1,16,256]{3,2,1,0:T(8,128)(2,1)}) %reduce-scatter.3.cloned.1.call-update) | async-done | bytes 8208 | tf_op jit(solution)/shard_map/reduce_scatter | solution.py:141
  191.7 1.4 fusion.24
  (42 shorter events, 0.2 us)
Async XLA Ops:
  7.2 120.7 %copy-start = (bf16[2,256,2048]{2,1,0:T(8,128)(2,1)S(1)}, bf16[2,256,2048]{2,1,0:T(8,128)(2,1)}, u32[]{:S(2)}) copy-start(bf16[2,256,2048]{2,1,0:T(8,128)(2,1)} %param.46) | copy-start | bytes 6291460
  7.2 4.3 %copy-start.3 = (bf16[256,512]{1,0:T(8,128)(2,1)S(1)}, bf16[256,512]{1,0:T(8,128)(2,1)}, u32[]{:S(2)}) copy-start(bf16[256,512]{1,0:T(8,128)(2,1)} %param.32) | copy-start | bytes 786436
  7.2 4.4 %copy-start.4 = (bf16[256,512]{1,0:T(8,128)(2,1)S(1)}, bf16[256,512]{1,0:T(8,128)(2,1)}, u32[]{:S(2)}) copy-start(bf16[256,512]{1,0:T(8,128)(2,1)} %param.33) | copy-start | bytes 786436
  7.2 4.6 %copy-start.14 = (f32[8]{0:T(128)S(1)}, f32[8]{0:T(128)}, u32[]{:S(2)}) copy-start(f32[8]{0:T(128)} %param.35) | copy-start | bytes 100
  7.2 4.6 %copy-start.13 = (f32[16,8]{0,1:T(8,128)S(1)}, f32[16,8]{0,1:T(8,128)}, u32[]{:S(2)}) copy-start(f32[16,8]{0,1:T(8,128)} %param.36) | copy-start | bytes 1540
  7.2 4.6 %copy-start.15 = (f32[8]{0:T(128)S(1)}, f32[8]{0:T(128)}, u32[]{:S(2)}) copy-start(f32[8]{0:T(128)} %param.34) | copy-start | bytes 100
  7.2 4.6 %copy-start.12 = (bf16[2048,8]{0,1:T(8,128)(2,1)S(1)}, bf16[2048,8]{0,1:T(8,128)(2,1)}, u32[]{:S(2)}) copy-start(bf16[2048,8]{0,1:T(8,128)(2,1)} %param.31) | copy-start | bytes 98308
  7.2 106.6 %all-reduce.3.cloned.1.call-start = ((), (), s32[]{:S(2)}) async-start(), calls=%async_computation.4 | async-start | bytes 131072 | tf_op jit(solution)/shard_map/psum | solution.py:109
  9.4 4.6 %copy-start.8 = (bf16[4,512]{1,0:T(4,128)(2,1)S(1)}, bf16[4,512]{1,0:T(4,128)(2,1)}, u32[]{:S(2)}) copy-start(bf16[4,512]{1,0:T(4,128)(2,1)} %param.37) | copy-start | bytes 12292
  9.4 4.7 %copy-start.5 = (bf16[16,3,512]{2,0,1:T(8,128)(2,1)S(1)}, bf16[16,3,512]{2,0,1:T(8,128)(2,1)}, u32[]{:S(2)}) copy-start(bf16[16,3,512]{2,0,1:T(8,128)(2,1)} %param.38) | copy-start | bytes 147460
  11.4 2.8 %copy-start.9 = (f32[512]{0:T(512)S(1)}, f32[512]{0:T(512)}, u32[]{:S(2)}) copy-start(f32[512]{0:T(512)} %param.41) | copy-start | bytes 6148
  47.8 9.8 %copy-start.1 = (f32[16,8,64,128]{3,2,1,0:T(8,128)}, f32[16,8,64,128]{3,2,1,0:T(8,128)S(1)}, u32[]{:S(2)}) copy-start(f32[16,8,64,128]{3,2,1,0:T(8,128)S(1)} %multiply_add_fusion) | copy-start | bytes 12582916
  47.8 9.9 %copy-start.11 = (f32[8]{0:T(128)S(1)}, f32[8]{0:T(128)}, u32[]{:S(2)}) copy-start(f32[8]{0:T(128)} %param.40) | copy-start | bytes 100
  57.6 3.1 %copy-start.7 = (s32[16,4]{0,1:T(4,128)S(1)}, s32[16,4]{0,1:T(4,128)}, u32[]{:S(2)}) copy-start(s32[16,4]{0,1:T(4,128)} %param.26) | copy-start | bytes 772
  57.6 56.2 %copy-start.2 = (bf16[16,2048]{1,0:T(8,128)(2,1)S(1)}, bf16[16,2048]{1,0:T(8,128)(2,1)}, u32[]{:S(2)}) copy-start(bf16[16,2048]{1,0:T(8,128)(2,1)} %param.25) | copy-start | bytes 196612
  57.7 57.2 %copy-start.6 = (f32[2048]{0:T(1024)S(1)}, f32[2048]{0:T(1024)}, u32[]{:S(2)}) copy-start(f32[2048]{0:T(1024)} %param.43) | copy-start | bytes 24580
  60.7 100.1 %reduce-scatter.5.cloned.1.call-start = ((), (), s32[]{:S(2)}) async-start(), calls=%async_computation.6 | async-start | bytes 589824 | tf_op jit(solution)/shard_map/reduce_scatter | solution.py:138
  131.1 4.6 %copy-start.10 = (f32[16,4]{0,1:T(4,128)S(1)}, f32[16,4]{0,1:T(4,128)}, u32[]{:S(2)}) copy-start(f32[16,4]{0,1:T(4,128)} %param.27) | copy-start | bytes 772
  131.1 60.5 %reduce-scatter.3.cloned.1.call-start = ((), (), s32[]{:S(2)}) async-start(), calls=%async_computation.5 | async-start | bytes 73728 | tf_op jit(solution)/shard_map/reduce_scatter | solution.py:141
  162.2 29.4 %all-to-all-start.1 = ((bf16[4,2,16,256]{3,2,1,0:T(8,128)(2,1)}), bf16[4,2,16,256]{3,2,1,0:T(8,128)(2,1)S(1)}, u32[]{:S(2)}, u32[]{:S(2)}) async-start(bf16[4,2,16,256]{3,2,1,0:T(8,128)(2,1)} %copy.64), calls=%async_computation.3 | async-start | bytes 131072 | tf_op jit(solution)/shard_map/all_to_all | solution.py:149
Sparse Core Ops, SparseCore 0:
  60.8 53.0 all-reduce.2
  131.3 29.4 reduce-scatter.4
  163.0 28.6 reduce-scatter.2
where the time goes:
time: 200 us
  waiting for transfers between devices  103 us (52%)
  blocking collectives  40.9 us (20%)
  matrix products  28.4 us (14%)
  between operations  14 us (7%)
  other arithmetic  7.67 us (4%)
  starting transfers between devices  3.77 us (2%)
  local copies, waits for them, and re-layouts  2.39 us (1%)
    psum x1, waiting for transfers between devices, on_device(): mixed = lax.psum(mixer_part.astype(jnp.bfloat16), 'tp')  52.3 us
    psum x1, blocking collectives, on_device(): lax.psum(write_part.astype(jnp.bfloat16), 'tp').astype(jnp.float32)  30.3 us
    reduce_scatter x1, waiting for transfers between devices, on_device(): lax.psum_scatter(shared_part.reshape(1, 1, seq_rows, model_width).astype(...  25.2 us
    reduce_scatter x1, waiting for transfers between devices, on_device(): lax.psum_scatter(terms.astype(jnp.bfloat16), 'tp', scatter_dimension=3, t...  25 us
    all_to_all x1, blocking collectives, on_device(): lax.all_to_all(send_rows, 'ep', split_axis=0, concat_axis=0, tiled=True)  10.6 us
    dot_general x1, matrix products, on_device(): jnp.einsum('shpn,sn->shp', new_state, read_vec, precision=lax.Precision.H...  9.81 us
  transfers between devices with their start and end apart: 4, of which 3 were waited for; matrix products, arithmetic and copies ran while one was open for 4% of the time, Pallas kernels for 0%

commit v1 on v0

--- a/solution.py
+++ b/solution.py
@@ -106,7 +106,7 @@
     gated = rms_normed(readout * jax.nn.silu(gate_heads), head_gain.reshape(heads_here, HEAD_DIM))
     gated = gated.astype(jnp.bfloat16).reshape(seq_rows, heads_here * HEAD_DIM)
     mixer_part = jnp.dot(gated, output_weight, preferred_element_type=jnp.float32)
-    mixed = lax.psum(mixer_part.astype(jnp.bfloat16), "tp")
+    mixed = jnp.sum(lax.all_gather(mixer_part.astype(jnp.bfloat16), "tp"), axis=0)
     resid = (tokens_f + mixed.astype(jnp.float32)).astype(jnp.bfloat16)
     normed_ffn = rms_normed(resid.astype(jnp.float32), channel_gain).astype(jnp.bfloat16)
     resid_own = lax.dynamic_slice_in_dim(resid, col_start, col_count, 1)

time: 200 us -> 164 us (0.82)
  waiting for transfers between devices: 103 us -> 49 us
  blocking collectives: 40.9 us -> 57.8 us
    psum x1 -> x0, waiting for transfers between devices: 52.3 us -> none  [on_device(): mixed = lax.psum(mixer_part.astype(jnp.bfloat16), 'tp')]
    all_gather x0 -> x1, blocking collectives: none -> 14.9 us  [on_device(): lax.all_gather(mixer_part.astype(jnp.bfloat16), 'tp')]
  transfers between devices with their start and end apart: 4 -> 3, of which waited for: 3 -> 2; matrix products, arithmetic and copies ran while one was open for 4% -> 4% of each run, Pallas kernels for 0% -> 0%
where the time goes in v1:
time: 164 us; the launch traced here: 163 us
  blocking collectives  57.8 us (35%)
  waiting for transfers between devices  49 us (30%)
  matrix products  27.8 us (17%)
  between operations  14.3 us (9%)
  other arithmetic  7.45 us (5%)
  starting transfers between devices  3.58 us (2%)
  local copies, waits for them, and re-layouts  3.21 us (2%)
    psum x1, blocking collectives, on_device(): lax.psum(write_part.astype(jnp.bfloat16), 'tp').astype(jnp.float32)  30.3 us
    reduce_scatter x1, waiting for transfers between devices, on_device(): lax.psum_scatter(shared_part.reshape(1, 1, seq_rows, model_width).astype(...  25.3 us
    reduce_scatter x1, waiting for transfers between devices, on_device(): lax.psum_scatter(terms.astype(jnp.bfloat16), 'tp', scatter_dimension=3, t...  23.7 us
    all_gather x1, blocking collectives, on_device(): lax.all_gather(mixer_part.astype(jnp.bfloat16), 'tp')  14.9 us
    all_to_all x1, blocking collectives, on_device(): lax.all_to_all(send_rows, 'ep', split_axis=0, concat_axis=0, tiled=True)  12.5 us
    dot_general x1, matrix products, on_device(): jnp.einsum('shpn,sn->shp', new_state, read_vec, precision=lax.Precision.H...  9.81 us
    all_to_all x1, starting transfers between devices, on_device(): lax.all_to_all(expert_rows, 'ep', split_axis=0, concat_axis=0, tiled=True)  3.5 us
    dot_general x1, matrix products, expert_terms(): jnp.einsum('ajcf,jfd->ajcd', hidden, expert_down, preferred_element_type=...  3.28 us
  transfers between devices with their start and end apart: 3, of which 2 were waited for; matrix products, arithmetic and copies ran while one was open for 4% of the time, Pallas kernels for 0%

profile of v1, /device:TPU:0, one launch (start us, length us, event | category | flops | bytes accessed | tf_op | source)
XLA Modules:
  0.0 163.2 jit_solution(2125472602924894963)
XLA Ops:
  7.2 0.0 reduce-scatter.5.cloned.1.call-start
  7.3 0.9 copy.60
  8.2 0.1 eq.20
  8.3 0.1 fusion.42
  8.4 0.1 reduce_window_sum.11
  8.5 0.2 select_reduce_fusion.1
  8.7 0.1 reduce_sum.86
  8.7 0.1 copy.61
  8.8 0.7 multiply_add_fusion.1
  9.5 0.1 convert_reduce_fusion
  9.6 1.0 fusion.31
  10.6 0.9 fusion.33
  11.5 2.0 %fusion.21 = f32[16,512]{1,0:T(8,128)S(1)} fusion(bf16[16,2048]{1,0:T(8,128)(2,1)S(1)} %fusion.33, bf16[2048,512]{1,0:T(8,128)(2,1)} %param.29), kind=kOutput, calls=%fused_computation.17 | convolution fusion | flops 33570816 | bytes 2195456 | tf_op jit(solution)/shard_map/dot_general | solution.py:81
  13.5 0.1 reshape.93
  13.6 0.1 convolution_convert_fusion.6
  13.8 0.2 convolution_convert_fusion.5
  14.0 0.1 subtract_exponential_fusion
  14.1 0.1 copy.59
  14.2 2.0 %fusion.22 = bf16[16,1,512]{2,0,1:T(8,128)(2,1)S(1)} fusion(bf16[16,2048]{1,0:T(8,128)(2,1)S(1)} %fusion.33, bf16[2048,512]{1,0:T(8,128)(2,1)} %param.30), kind=kOutput, calls=%fused_computation.21 | convolution fusion | flops 33562624 | bytes 2179072 | tf_op jit(solution)/shard_map/dot_general | solution.py:84
  16.2 0.1 reduce_sum.81
  16.3 0.1 copy.58
  16.4 0.1 mul.206
  16.4 30.3 %all-reduce = (bf16[16,512]{1,0:T(8,128)(2,1)S(1)}, bf16[16,512]{1,0:T(8,128)(2,1)S(1)}) all-reduce(bf16[16,512]{1,0:T(8,128)(2,1)S(1)} %convolution_convert_fusion.6, bf16[16,512]{1,0:T(8,128)(2,1)S(1)} %convolution_convert_fusion.5), channel_id=1, replica_groups=mesh['ep'=4,'tp'=8] {'tp'}, use_global_device_ids=true, to_apply=%region_2.0 | all-reduce | flops 16384 | bytes 65536 | tf_op jit(solution)/shard_map/psum | solution.py:78
  46.7 0.1 broadcast_multiply_fusion
  46.9 3.1 %multiply_add_fusion = f32[16,8,64,128]{3,2,1,0:T(8,128)S(1)} fusion(f32[16,8,64,128]{3,2,1,0:T(8,128)} %param.39, f32[16,128]{1,0:T(8,128)S(1)} %get-tuple-element.12, f32[16,8,64]{2,1,0:T(8,128)S(1)} %broadcast_multiply_fusion, f32[16,8]{1,0:T(8,128)S(1)} %copy.58), kind=kLoop, calls=%fused_computation | loop fusion | flops 3145728 | bytes 8430080 | tf_op jit(solution)/shard_map/add | solution.py:100
  50.0 9.8 %fusion.68 = f32[16,1,8,64]{3,1,2,0:T(1,128)S(1)} fusion(f32[16,8,64,128]{3,2,1,0:T(8,128)S(1)} %multiply_add_fusion, f32[16,128,1,1]{1,2,3,0:T(1,128)S(1)} %bitcast.74), kind=kOutput, calls=%fused_computation.95 | convolution fusion | flops 12582912 | bytes 4235264 | tf_op jit(solution)/shard_map/shpn,sn->shp/dot_general | solution.py:103
  59.8 0.0 copy-start.6
  59.8 0.2 multiply_reduce_fusion.1
  60.0 0.1 multiply_convert_fusion
  60.1 0.1 reshape.89
  60.2 2.0 %convolution_convert_fusion.3 = bf16[16,2048]{1,0:T(8,128)(2,1)S(1)} fusion(bf16[16,512]{1,0:T(8,128)(2,1)S(1)} %reshape.89, bf16[512,2048]{1,0:T(8,128)(2,1)} %param.42), kind=kOutput, calls=%fused_computation.5 | convolution fusion | flops 33587200 | bytes 2179072 | tf_op jit(solution)/shard_map/dot_general | solution.py:108
  62.2 14.9 %all-gather = bf16[128,2048]{1,0:T(8,128)(2,1)S(1)} all-gather(bf16[16,2048]{1,0:T(8,128)(2,1)S(1)} %convolution_convert_fusion.3), channel_id=2, replica_groups=mesh['ep'=4,'tp'=8] {'tp'}, dimensions={0}, use_global_device_ids=true | all-gather | bytes 589824 | tf_op jit(solution)/shard_map/all_gather | solution.py:109
  77.1 0.1 reduce_sum.83
  77.2 0.1 fusion.28
  77.4 0.3 convolution_convert_fusion.1
  77.7 12.5 %all_to_all.10 = bf16[4,2,16,2048]{3,2,1,0:T(8,128)(2,1)S(1)} all-to-all(bf16[4,2,16,2048]{3,2,1,0:T(8,128)(2,1)S(1)} %bitcast.71), channel_id=1, replica_groups=mesh['ep'=4,'tp'=8] {'ep'}, dimensions={0} | all-to-all | bytes 1048576 | tf_op jit(solution)/shard_map/all_to_all | solution.py:132
  90.2 2.1 %fusion.7 = f32[4,2,16,256]{3,2,0,1:T(8,128)S(1)} fusion(bf16[2,2048,256]{2,1,0:T(8,128)(2,1)} %param.44, bf16[4,2,16,2048]{3,2,1,0:T(8,128)(2,1)S(1)} %all_to_all.10), kind=kOutput, calls=%fused_computation.12 | convolution fusion | flops 134217728 | bytes 2752512 | tf_op jit(solution)/shard_map/ajcd,jdf->ajcf/dot_general | solution.py:28
  92.3 3.3 %fusion = bf16[4,2,16,2048]{3,2,0,1:T(8,128)(2,1)} fusion(bf16[2,256,2048]{2,1,0:T(8,128)(2,1)S(1)} %copy-done, bf16[2,2048,256]{2,1,0:T(8,128)(2,1)} %param.45, bf16[4,2,16,2048]{3,2,1,0:T(8,128)(2,1)S(1)} %all_to_all.10, f32[4,2,16,256]{3,2,0,1:T(8,128)S(1)} %fusion.7), kind=kOutput, calls=%fused_computation.3 | convolution fusion | flops 268894208 | bytes 5373952 | tf_op jit(solution)/shard_map/ajcf,jfd->ajcd/dot_general | solution.py:35
  95.6 0.0 reduce-scatter.3.cloned.1.call-start
  95.7 1.5 fusion.65
  97.2 3.0 %fusion.1 = bf16[1,1,16,2048]{3,2,1,0:T(8,128)(2,1)} fusion(bf16[256,2048]{1,0:T(8,128)(2,1)} %param.49, bf16[2048,256]{1,0:T(8,128)(2,1)} %param.48, f32[16,256]{1,0:T(8,128)S(1)} %fusion.65, bf16[16,2048]{1,0:T(8,128)(2,1)S(1)} %get-tuple-element.6, f32[2048]{0:T(1024)S(1)} %copy-done.6, f32[16]{0:T(128)S(1)} %add_rsqrt_fusion.1), kind=kOutput, calls=%fused_computation.6 | convolution fusion | flops 33742848 | bytes 2252864 | tf_op jit(solution)/shard_map/dot_general | solution.py:117
  100.2 0.1 select_reduce_fusion
  100.3 23.7 %reduce-scatter.5.cloned.1.call-done = bf16[4,2,16,256]{3,2,0,1:T(8,128)(2,1)} async-done(((bf16[4,2,16,2048]{3,2,0,1:T(8,128)(2,1)}), bf16[4,2,16,256]{3,2,0,1:T(8,128)(2,1)}) %reduce-scatter.5.cloned.1.call-update) | async-done | bytes 65552 | tf_op jit(solution)/shard_map/reduce_scatter | solution.py:138
  124.0 1.5 copy.64
  125.5 3.5 %all-to-all-start.1 = ((bf16[4,2,16,256]{3,2,1,0:T(8,128)(2,1)}), bf16[4,2,16,256]{3,2,1,0:T(8,128)(2,1)S(1)}, u32[]{:S(2)}, u32[]{:S(2)}) async-start(bf16[4,2,16,256]{3,2,1,0:T(8,128)(2,1)} %copy.64), calls=%async_computation.3 | async-start | bytes 131072 | tf_op jit(solution)/shard_map/all_to_all | solution.py:149
  129.0 0.6 fusion.41
  129.6 25.3 %reduce-scatter.3.cloned.1.call-done = bf16[1,1,16,256]{3,2,1,0:T(8,128)(2,1)} async-done(((bf16[1,1,16,2048]{3,2,1,0:T(8,128)(2,1)}), bf16[1,1,16,256]{3,2,1,0:T(8,128)(2,1)}) %reduce-scatter.3.cloned.1.call-update) | async-done | bytes 8208 | tf_op jit(solution)/shard_map/reduce_scatter | solution.py:141
  154.9 1.4 fusion.24
  (39 shorter events, 0.2 us)
Async XLA Ops:
  7.2 85.1 %copy-start = (bf16[2,256,2048]{2,1,0:T(8,128)(2,1)S(1)}, bf16[2,256,2048]{2,1,0:T(8,128)(2,1)}, u32[]{:S(2)}) copy-start(bf16[2,256,2048]{2,1,0:T(8,128)(2,1)} %param.46) | copy-start | bytes 6291460
  7.2 6.4 %copy-start.3 = (bf16[256,512]{1,0:T(8,128)(2,1)S(1)}, bf16[256,512]{1,0:T(8,128)(2,1)}, u32[]{:S(2)}) copy-start(bf16[256,512]{1,0:T(8,128)(2,1)} %param.32) | copy-start | bytes 786436
  7.2 6.6 %copy-start.4 = (bf16[256,512]{1,0:T(8,128)(2,1)S(1)}, bf16[256,512]{1,0:T(8,128)(2,1)}, u32[]{:S(2)}) copy-start(bf16[256,512]{1,0:T(8,128)(2,1)} %param.33) | copy-start | bytes 786436
  7.2 6.7 %copy-start.13 = (f32[8]{0:T(128)S(1)}, f32[8]{0:T(128)}, u32[]{:S(2)}) copy-start(f32[8]{0:T(128)} %param.35) | copy-start | bytes 100
  7.2 6.7 %copy-start.12 = (f32[16,8]{0,1:T(8,128)S(1)}, f32[16,8]{0,1:T(8,128)}, u32[]{:S(2)}) copy-start(f32[16,8]{0,1:T(8,128)} %param.36) | copy-start | bytes 1540
  7.2 6.7 %copy-start.14 = (f32[8]{0:T(128)S(1)}, f32[8]{0:T(128)}, u32[]{:S(2)}) copy-start(f32[8]{0:T(128)} %param.34) | copy-start | bytes 100
  7.2 6.7 %copy-start.11 = (bf16[2048,8]{0,1:T(8,128)(2,1)S(1)}, bf16[2048,8]{0,1:T(8,128)(2,1)}, u32[]{:S(2)}) copy-start(bf16[2048,8]{0,1:T(8,128)(2,1)} %param.31) | copy-start | bytes 98308
  7.2 116.8 %reduce-scatter.5.cloned.1.call-start = ((), (), s32[]{:S(2)}) async-start(), calls=%async_computation.5 | async-start | bytes 589824 | tf_op jit(solution)/shard_map/reduce_scatter | solution.py:138
  11.5 4.6 %copy-start.7 = (bf16[4,512]{1,0:T(4,128)(2,1)S(1)}, bf16[4,512]{1,0:T(4,128)(2,1)}, u32[]{:S(2)}) copy-start(bf16[4,512]{1,0:T(4,128)(2,1)} %param.37) | copy-start | bytes 12292
  11.5 4.7 %copy-start.5 = (bf16[16,3,512]{2,0,1:T(8,128)(2,1)S(1)}, bf16[16,3,512]{2,0,1:T(8,128)(2,1)}, u32[]{:S(2)}) copy-start(bf16[16,3,512]{2,0,1:T(8,128)(2,1)} %param.38) | copy-start | bytes 147460
  13.5 2.8 %copy-start.8 = (f32[512]{0:T(512)S(1)}, f32[512]{0:T(512)}, u32[]{:S(2)}) copy-start(f32[512]{0:T(512)} %param.41) | copy-start | bytes 6148
  49.9 9.8 %copy-start.1 = (f32[16,8,64,128]{3,2,1,0:T(8,128)}, f32[16,8,64,128]{3,2,1,0:T(8,128)S(1)}, u32[]{:S(2)}) copy-start(f32[16,8,64,128]{3,2,1,0:T(8,128)S(1)} %multiply_add_fusion) | copy-start | bytes 12582916
  50.0 9.9 %copy-start.10 = (f32[8]{0:T(128)S(1)}, f32[8]{0:T(128)}, u32[]{:S(2)}) copy-start(f32[8]{0:T(128)} %param.40) | copy-start | bytes 100
  59.8 17.4 %copy-start.2 = (bf16[16,2048]{1,0:T(8,128)(2,1)S(1)}, bf16[16,2048]{1,0:T(8,128)(2,1)}, u32[]{:S(2)}) copy-start(bf16[16,2048]{1,0:T(8,128)(2,1)} %param.25) | copy-start | bytes 196612
  59.8 17.6 %copy-start.6 = (f32[2048]{0:T(1024)S(1)}, f32[2048]{0:T(1024)}, u32[]{:S(2)}) copy-start(f32[2048]{0:T(1024)} %param.43) | copy-start | bytes 24580
  95.6 4.6 %copy-start.9 = (f32[16,4]{0,1:T(4,128)S(1)}, f32[16,4]{0,1:T(4,128)}, u32[]{:S(2)}) copy-start(f32[16,4]{0,1:T(4,128)} %param.27) | copy-start | bytes 772
  95.6 59.3 %reduce-scatter.3.cloned.1.call-start = ((), (), s32[]{:S(2)}) async-start(), calls=%async_computation.4 | async-start | bytes 73728 | tf_op jit(solution)/shard_map/reduce_scatter | solution.py:141
  125.5 29.4 %all-to-all-start.1 = ((bf16[4,2,16,256]{3,2,1,0:T(8,128)(2,1)}), bf16[4,2,16,256]{3,2,1,0:T(8,128)(2,1)S(1)}, u32[]{:S(2)}, u32[]{:S(2)}) async-start(bf16[4,2,16,256]{3,2,1,0:T(8,128)(2,1)} %copy.64), calls=%async_computation.3 | async-start | bytes 131072 | tf_op jit(solution)/shard_map/all_to_all | solution.py:149
Sparse Core Ops, SparseCore 0:
  95.7 28.2 reduce-scatter.4
  126.2 28.6 reduce-scatter.2
